TPU v7x, 32 devices: a whole 2x2x4 slice. The times are simulated.
32 devices in a mesh: grp: 2 (over y), ra: 4 (over z), cb: 4 (over x, core).
Axes of the slice: x: 2, y: 2, z: 4, core: 2. Of those that a mesh axis runs over, the one named last changes fastest.
Arguments:
- stream: bfloat16 [256, 4096], P('grp', 'ra'), parts along dimension 0, may hold values from -180 to 180
- w_gate: float32 [2, 4096, 11264], P(None, 'ra', 'cb'), may hold values from -0.09375 to 0.09375
- w_up: float32 [2, 4096, 11264], P(None, 'ra', 'cb'), may hold values from -0.09375 to 0.09375
- w_down: float32 [2, 11264, 4096], P(None, 'cb', 'ra'), may hold values from -0.0546875 to 0.0546875
- gate_scale: float32 [2, 11264], P(None, 'cb'), may hold values from 0.5 to 2
- up_scale: float32 [2, 11264], P(None, 'cb'), may hold values from 0.5 to 2
- down_scale: float32 [2, 4096], P(None, 'ra'), may hold values from 0.5 to 2
- pre_gain: float32 [2, 4096], P(None, 'ra'), may hold values from 0.1 to 1.9
- out_gain: float32 [4096], P('ra'), may hold values from 0.1 to 1.9
Outputs:
- normed: bfloat16 [256, 4096], P('grp', 'ra'), parts along dimension 0
There are 2 independent parts, one for each index of `grp`. A program takes and returns all parts, laid end to end along the dimension named above; an argument that names none is the same for every part. Nothing has to cross between parts.
All inputs are finite; a program needn't handle non-finite values.
Results may differ from a plain program's by a relative error of at most 0.018.
Values may be sent and summed in bfloat16 or wider, within the bound.
No kernel may reach another device: no remote copies, remote signals or barrier semaphores. Data moves between devices by JAX's collectives and lax.ppermute only.
A program may use at most 192 MiB of HBM per device.

v0:
```python
import jax
import jax.numpy as jnp
from jax import lax
from jax.sharding import PartitionSpec as P

D = 4096
LAYERS = 2


def local(stream, w_gate, w_up, w_down, gate_scale, up_scale, down_scale, pre_gain, out_gain):
    current = stream
    tokens = stream.shape[0]
    share = tokens // lax.axis_size("ra")
    for layer in range(LAYERS):
        xvals = current.astype(jnp.float32)
        squares = jnp.sum(xvals * xvals, axis=1)
        scaled = (xvals * pre_gain[layer]).astype(jnp.bfloat16)
        gate_part = jnp.dot(
            scaled, w_gate[layer].astype(jnp.bfloat16), preferred_element_type=jnp.float32
        )
        up_part = jnp.dot(
            scaled, w_up[layer].astype(jnp.bfloat16), preferred_element_type=jnp.float32
        )
        down_local = w_down[layer].astype(jnp.bfloat16)
        total = lax.psum(squares, "ra")
        operands = (gate_part, up_part)
        summed = (
            lax.psum_scatter(operands[0], "ra", scatter_dimension=0, tiled=True),
            lax.psum_scatter(operands[1], "ra", scatter_dimension=0, tiled=True),
        )
        own_rows = lax.dynamic_slice_in_dim(total, lax.axis_index("ra") * share, share)
        rinv = lax.rsqrt(own_rows / D + 1e-06)[:, None]
        gate = summed[0] * rinv * gate_scale[layer]
        upper = summed[1] * rinv * up_scale[layer]
        hidden = (jax.nn.silu(gate) * upper).astype(jnp.bfloat16)
        terms = jnp.dot(
            lax.all_gather(hidden, "ra", axis=0, tiled=True),
            down_local,
            preferred_element_type=jnp.float32,
        )
        branch = lax.psum(terms.astype(jnp.bfloat16), "cb").astype(jnp.float32) * down_scale[layer]
        current = (0.5 * xvals + branch).astype(jnp.bfloat16)
    xvals = current.astype(jnp.float32)
    final_sum = lax.psum(jnp.sum(xvals * xvals, axis=1), "ra")
    rinv = lax.rsqrt(final_sum / D + 1e-06)[:, None]
    return (xvals * rinv * out_gain).astype(jnp.bfloat16)


def solution(mesh):
    placed = (
        P("grp", "ra"),
        P(None, "ra", "cb"),
        P(None, "ra", "cb"),
        P(None, "cb", "ra"),
        P(None, "cb"),
        P(None, "cb"),
        P(None, "ra"),
        P(None, "ra"),
        P("ra"),
    )
    return jax.shard_map(
        local, mesh=mesh, in_specs=placed, out_specs=P("grp", "ra"), check_vma=False
    )
```

profile of v0, /device:TPU:0, one launch (start us, length us, event | category | flops | bytes accessed | tf_op | source)
XLA Modules:
  0.0 296.9 jit_solution(10310652706290276706)
XLA Ops:
  6.5 0.0 reduce-scatter.5.cloned.1.call-start
  6.5 0.8 fusion.24
  7.3 0.0 copy-start.2
  7.3 8.6 %convert.12 = bf16[2,1024,2816]{2,1,0:T(8,128)(2,1)S(1)} convert(f32[2,1024,2816]{2,1,0:T(8,128)} %param.10) | non-fusion elementwise | flops 5767168 | bytes 34603008 | tf_op jit(solution)/shard_map/convert.5
  15.9 0.0 copy-start.1
  15.9 4.2 %copy-done.1 = bf16[2,1024,2816]{2,1,0:T(8,128)(2,1)} copy-done((bf16[2,1024,2816]{2,1,0:T(8,128)(2,1)}, bf16[2,1024,2816]{2,1,0:T(8,128)(2,1)S(1)}, u32[]{:S(2)}) %copy-start.1) | copy-done | bytes 11534360
  20.1 0.0 copy-done.2
  20.1 2.0 fusion.5
  22.2 0.0 reduce-scatter.5.cloned.1.call-update
  22.2 0.0 reduce-scatter.7.cloned.1.call-start
  22.2 8.6 %convert.13 = bf16[2,1024,2816]{2,1,0:T(8,128)(2,1)S(1)} convert(f32[2,1024,2816]{2,1,0:T(8,128)} %param.11) | non-fusion elementwise | flops 5767168 | bytes 34603008 | tf_op jit(solution)/shard_map/convert.4
  30.8 0.0 copy-start
  30.8 4.2 %copy-done = bf16[2,1024,2816]{2,1,0:T(8,128)(2,1)} copy-done((bf16[2,1024,2816]{2,1,0:T(8,128)(2,1)}, bf16[2,1024,2816]{2,1,0:T(8,128)(2,1)S(1)}, u32[]{:S(2)}) %copy-start) | copy-done | bytes 11534360
  35.0 2.1 fusion.4
  37.1 0.0 reduce-scatter.7.cloned.1.call-update
  37.1 0.0 all-reduce.3.cloned.1.call-start
  37.2 0.0 copy-start.3
  37.2 0.0 copy-start.4
  37.2 12.6 %convert.14 = bf16[2,2816,1024]{2,1,0:T(8,128)(2,1)} convert(f32[2,2816,1024]{2,1,0:T(8,128)} %param.12) | non-fusion elementwise | flops 5767168 | bytes 34603008 | tf_op jit(solution)/shard_map/convert.3
  49.8 0.0 copy-start.5
  49.8 0.1 fusion.14
  50.0 13.6 %psum.35 = f32[128]{0:T(128)S(1)} all-reduce(f32[128]{0:T(128)S(1)} %fusion.14), channel_id=1, replica_groups=mesh['grp'=2,'ra'=4,'cb'=4] {'ra'}, use_global_device_ids=true, to_apply=%region_2.0 | all-reduce | flops 128 | bytes 1024 | tf_op jit(solution)/shard_map/psum | solution.py:25
  63.6 0.1 add_rsqrt_fusion.2
  63.7 0.0 copy-done.3
  63.7 0.0 copy-done.4
  63.7 0.1 slice_reduce_fusion
  63.8 0.0 reduce-scatter.5.cloned.1.call-done
  63.8 29.2 %reduce-scatter.7.cloned.1.call-done = f32[32,2816]{1,0:T(8,128)} async-done(((f32[128,2816]{1,0:T(8,128)}), f32[32,2816]{1,0:T(8,128)}) %reduce-scatter.7.cloned.1.call-update) | async-done | bytes 360464 | tf_op jit(solution)/shard_map/reduce_scatter | solution.py:29
  93.0 1.3 multiply_convert_fusion.1
  94.3 17.2 %all_gather.6 = bf16[128,2816]{1,0:T(8,128)(2,1)S(1)} all-gather(bf16[32,2816]{1,0:T(8,128)(2,1)S(1)} %multiply_convert_fusion.1), channel_id=1, replica_groups=mesh['grp'=2,'ra'=4,'cb'=4] {'ra'}, dimensions={0}, use_global_device_ids=true | all-gather | bytes 901120 | tf_op jit(solution)/shard_map/all_gather | solution.py:37
  111.5 4.3 %fusion.6 = bf16[128,1024]{1,0:T(8,128)(2,1)} fusion(bf16[128,2816]{1,0:T(8,128)(2,1)S(1)} %all_gather.6, bf16[2,2816,1024]{2,1,0:T(8,128)(2,1)} %convert.14), kind=kOutput, calls=%fused_computation.12 | convolution fusion | flops 738328576 | bytes 6750208 | tf_op jit(solution)/shard_map/dot_general | solution.py:36
  115.8 0.0 all-reduce.3.cloned.1.call-update
  115.8 0.0 reduce-scatter.9.cloned.1.call-start
  115.9 0.0 copy-done.5
  115.9 31.3 %all-reduce.3.cloned.1.call-done = bf16[128,1024]{1,0:T(8,128)(2,1)} async-done(((bf16[128,1024]{1,0:T(8,128)(2,1)}), bf16[128,1024]{1,0:T(8,128)(2,1)}) %all-reduce.3.cloned.1.call-update) | async-done | bytes 262160 | tf_op jit(solution)/shard_map/psum | solution.py:41
  147.2 1.2 fusion.18
  148.4 4.7 %fusion.2 = f32[128,2816]{1,0:T(8,128)} fusion(bf16[2,1024,2816]{2,1,0:T(8,128)(2,1)} %copy-done.1, bf16[128,1024]{1,0:T(8,128)(2,1)S(1)} %get-tuple-element.10, f32[1024]{0:T(1024)S(1)} %bitcast.31), kind=kOutput, calls=%fused_computation.5 | convolution fusion | flops 738590720 | bytes 7475200 | tf_op jit(solution)/shard_map/dot_general | solution.py:18
  153.1 0.0 reduce-scatter.9.cloned.1.call-update
  153.1 0.0 reduce-scatter.11.cloned.1.call-start
  153.1 4.7 %fusion.1 = f32[128,2816]{1,0:T(8,128)} fusion(bf16[2,1024,2816]{2,1,0:T(8,128)(2,1)} %copy-done, bf16[128,1024]{1,0:T(8,128)(2,1)S(1)} %get-tuple-element.10, f32[1024]{0:T(1024)S(1)} %bitcast.32), kind=kOutput, calls=%fused_computation.3 | convolution fusion | flops 738590720 | bytes 7475200 | tf_op jit(solution)/shard_map/dot_general | solution.py:21
  157.8 0.0 reduce-scatter.11.cloned.1.call-update
  157.8 0.0 copy-start.6
  157.9 0.0 all-reduce.5.cloned.1.call-start
  157.9 12.3 %psum.37 = f32[128]{0:T(128)S(1)} all-reduce(f32[128]{0:T(128)S(1)} %get-tuple-element.9), channel_id=1, replica_groups=mesh['grp'=2,'ra'=4,'cb'=4] {'ra'}, use_global_device_ids=true, to_apply=%region_7.8 | all-reduce | flops 128 | bytes 1024 | tf_op jit(solution)/shard_map/psum | solution.py:25
  170.2 0.1 add_rsqrt_fusion.1
  170.3 16.5 %reduce-scatter.9.cloned.1.call-done = f32[32,2816]{1,0:T(8,128)} async-done(((f32[128,2816]{1,0:T(8,128)}), f32[32,2816]{1,0:T(8,128)}) %reduce-scatter.9.cloned.1.call-update) | async-done | bytes 360464 | tf_op jit(solution)/shard_map/reduce_scatter | solution.py:28
  186.8 34.4 %reduce-scatter.11.cloned.1.call-done = f32[32,2816]{1,0:T(8,128)} async-done(((f32[128,2816]{1,0:T(8,128)}), f32[32,2816]{1,0:T(8,128)}) %reduce-scatter.11.cloned.1.call-update) | async-done | bytes 360464 | tf_op jit(solution)/shard_map/reduce_scatter | solution.py:29
  221.2 1.3 multiply_convert_fusion
  222.5 17.2 %all_gather.7 = bf16[128,2816]{1,0:T(8,128)(2,1)S(1)} all-gather(bf16[32,2816]{1,0:T(8,128)(2,1)S(1)} %multiply_convert_fusion), channel_id=1, replica_groups=mesh['grp'=2,'ra'=4,'cb'=4] {'ra'}, dimensions={0}, use_global_device_ids=true | all-gather | bytes 901120 | tf_op jit(solution)/shard_map/all_gather | solution.py:37
  239.6 4.3 %fusion.7 = bf16[128,1024]{1,0:T(8,128)(2,1)} fusion(bf16[128,2816]{1,0:T(8,128)(2,1)S(1)} %all_gather.7, bf16[2,2816,1024]{2,1,0:T(8,128)(2,1)} %convert.14), kind=kOutput, calls=%fused_computation.13 | convolution fusion | flops 738328576 | bytes 6750208 | tf_op jit(solution)/shard_map/dot_general | solution.py:36
  244.0 0.0 all-reduce.5.cloned.1.call-update
  244.0 31.5 %all-reduce.5.cloned.1.call-done = bf16[128,1024]{1,0:T(8,128)(2,1)} async-done(((bf16[128,1024]{1,0:T(8,128)(2,1)}), bf16[128,1024]{1,0:T(8,128)(2,1)}) %all-reduce.5.cloned.1.call-update) | async-done | bytes 262160 | tf_op jit(solution)/shard_map/psum | solution.py:41
  275.5 1.2 fusion.8
  276.6 11.7 %psum.39 = f32[128]{0:T(128)S(1)} all-reduce(f32[128]{0:T(128)S(1)} %fusion.8), channel_id=1, replica_groups=mesh['grp'=2,'ra'=4,'cb'=4] {'ra'}, use_global_device_ids=true, to_apply=%region_11.12 | all-reduce | flops 128 | bytes 1024 | tf_op jit(solution)/shard_map/psum | solution.py:44
  288.3 0.0 copy-done.6
  288.3 1.8 fusion.10
  (2 shorter events, 0.0 us)
Async XLA Ops:
  6.5 57.3 %reduce-scatter.5.cloned.1.call-start = ((), (), s32[]{:S(2)}) async-start(), calls=%async_computation.4 | async-start | bytes 1802240 | tf_op jit(solution)/shard_map/reduce_scatter | solution.py:28
  7.3 12.8 %copy-start.2 = (bf16[128,1024]{1,0:T(8,128)(2,1)S(1)}, bf16[128,1024]{1,0:T(8,128)(2,1)}, u32[]{:S(2)}) copy-start(bf16[128,1024]{1,0:T(8,128)(2,1)} %param.9) | copy-start | bytes 786436
  15.9 4.2 %copy-start.1 = (bf16[2,1024,2816]{2,1,0:T(8,128)(2,1)}, bf16[2,1024,2816]{2,1,0:T(8,128)(2,1)S(1)}, u32[]{:S(2)}) copy-start(bf16[2,1024,2816]{2,1,0:T(8,128)(2,1)S(1)} %convert.12) | copy-start | bytes 34603012
  22.2 70.9 %reduce-scatter.7.cloned.1.call-start = ((), (), s32[]{:S(2)}) async-start(), calls=%async_computation.5 | async-start | bytes 1802240 | tf_op jit(solution)/shard_map/reduce_scatter | solution.py:29
  30.8 4.2 %copy-start = (bf16[2,1024,2816]{2,1,0:T(8,128)(2,1)}, bf16[2,1024,2816]{2,1,0:T(8,128)(2,1)S(1)}, u32[]{:S(2)}) copy-start(bf16[2,1024,2816]{2,1,0:T(8,128)(2,1)S(1)} %convert.13) | copy-start | bytes 34603012
  37.1 110.1 %all-reduce.3.cloned.1.call-start = ((), (), s32[]{:S(2)}) async-start(), calls=%async_computation.6 | async-start | bytes 524288 | tf_op jit(solution)/shard_map/psum | solution.py:41
  37.2 26.5 %copy-start.3 = (f32[2,2816]{1,0:T(2,128)S(1)}, f32[2,2816]{1,0:T(2,128)}, u32[]{:S(2)}) copy-start(f32[2,2816]{1,0:T(2,128)} %param.14) | copy-start | bytes 67588
  37.2 26.5 %copy-start.4 = (f32[2,2816]{1,0:T(2,128)S(1)}, f32[2,2816]{1,0:T(2,128)}, u32[]{:S(2)}) copy-start(f32[2,2816]{1,0:T(2,128)} %param.13) | copy-start | bytes 67588
  49.8 66.1 %copy-start.5 = (f32[2,1024]{1,0:T(2,128)S(1)}, f32[2,1024]{1,0:T(2,128)}, u32[]{:S(2)}) copy-start(f32[2,1024]{1,0:T(2,128)} %param.15) | copy-start | bytes 24580
  115.8 71.0 %reduce-scatter.9.cloned.1.call-start = ((), (), s32[]{:S(2)}) async-start(), calls=%async_computation.7 | async-start | bytes 1802240 | tf_op jit(solution)/shard_map/reduce_scatter | solution.py:28
  153.1 68.1 %reduce-scatter.11.cloned.1.call-start = ((), (), s32[]{:S(2)}) async-start(), calls=%async_computation.8 | async-start | bytes 1802240 | tf_op jit(solution)/shard_map/reduce_scatter | solution.py:29
  157.8 130.5 %copy-start.6 = (f32[1024]{0:T(1024)S(1)}, f32[1024]{0:T(1024)}, u32[]{:S(2)}) copy-start(f32[1024]{0:T(1024)} %param.17) | copy-start | bytes 12292
  157.9 117.6 %all-reduce.5.cloned.1.call-start = ((), (), s32[]{:S(2)}) async-start(), calls=%async_computation.9 | async-start | bytes 524288 | tf_op jit(solution)/shard_map/psum | solution.py:41
Sparse Core Ops, SparseCore 0:
  22.3 36.0 reduce-scatter.4
  60.8 32.2 reduce-scatter.6
  116.0 31.2 all-reduce.2
  153.2 33.5 reduce-scatter.8
  189.0 32.1 reduce-scatter.10
  244.1 31.3 all-reduce.4
where the time goes:
time: 298 us; the launch traced here: 297 us
  waiting for transfers between devices  143 us (48%)
  blocking collectives  71.9 us (24%)
  other arithmetic  36.8 us (12%)
  matrix products  22 us (7%)
  between operations  13.6 us (5%)
  local copies, waits for them, and re-layouts  9.34 us (3%)
    reduce_scatter x2, waiting for transfers between devices, local(): lax.psum_scatter(operands[1], 'ra', scatter_dimension=0, tiled=True)  63.6 us
    psum x2, waiting for transfers between devices, local(): lax.psum(terms.astype(jnp.bfloat16), 'cb').astype(jnp.float32)  62.8 us
    all_gather x2, blocking collectives, local(): lax.all_gather(hidden, 'ra', axis=0, tiled=True)  34.3 us
    another operation x3, other arithmetic  29.8 us
    psum x2, blocking collectives, local(): total = lax.psum(squares, 'ra')  25.9 us
    reduce_scatter x2, waiting for transfers between devices, local(): lax.psum_scatter(operands[0], 'ra', scatter_dimension=0, tiled=True)  16.6 us
    psum x1, blocking collectives, local(): final_sum = lax.psum(jnp.sum(xvals * xvals, axis=1), 'ra')  11.7 us
    dot_general x2, matrix products, local(): jnp.dot(lax.all_gather(hidden, 'ra', axis=0, tiled=True), down_local, pre...  8.61 us
  transfers between devices with their start and end apart: 6, of which 5 were waited for; matrix products, arithmetic and copies ran while one was open for 10% of the time, Pallas kernels for 0%

commit v1 on v0

v1 whole, which is shorter than its diff:
```python
import jax
import jax.numpy as jnp
from jax import lax
from jax.experimental import pallas as pl
from jax.experimental.pallas import tpu as pltpu
from jax.sharding import PartitionSpec as P


CHUNKS = 2
LANES = 128
BF = jnp.bfloat16
F32 = jnp.float32


def shift(value, axis, step):
    size = lax.axis_size(axis)
    return lax.ppermute(value, axis, [(i, (i + step) % size) for i in range(size)])


def swap(value, axis, bit):
    size = lax.axis_size(axis)
    return lax.ppermute(value, axis, [(i, i ^ bit) for i in range(size)])


def stages(axis):
    return [1 << s for s in range(lax.axis_size(axis).bit_length() - 1)]


def column_block(extent):
    for size in (256, 128):
        if extent % size == 0:
            return size
    return extent


def chunk_bounds(blocks):
    count = min(CHUNKS, blocks)
    edges = [-(-blocks * c // count) for c in range(count + 1)]
    return list(zip(edges[:-1], edges[1:]))


def two_floats(value):
    high = lax.reduce_precision(value, 8, 7)
    middle = lax.reduce_precision(value - high, 8, 7)
    low = value - high - middle
    lane = lax.broadcasted_iota(jnp.int32, (value.shape[0], LANES), 1)
    picked = jnp.where(lane == 0, high, jnp.where(lane == 1, middle, jnp.where(lane == 2, low, 0.0)))
    return picked.astype(BF)


def fetch(copies):
    for copy in copies:
        copy.start()
    return copies


def gate_up_kernel(x_ref, wg_hbm, wu_hbm, extra_ref, *rest, layer, lo, blk, cut, tail):
    outs, (buf, sems) = rest[:-2], rest[-2:]
    count = cut // blk
    copies = fetch(
        [
            pltpu.make_async_copy(w.at[layer, :, pl.ds((lo + j) * blk, blk)], buf.at[j, i], sems.at[j, i])
            for j in range(count)
            for i, w in enumerate((wg_hbm, wu_hbm))
        ]
    )
    rows = x_ref.shape[0] // len(outs)
    if tail:
        for i, out in enumerate(outs):
            out[:, 2 * cut :] = extra_ref[i * rows : (i + 1) * rows]
    x = x_ref[...]
    for j in range(count):
        for i in range(2):
            copies[2 * j + i].wait()
            value = jnp.dot(x, buf[j, i].astype(BF), preferred_element_type=F32).astype(BF)
            at = i * cut + j * blk
            for p, out in enumerate(outs):
                out[:, at : at + blk] = value[p * rows : (p + 1) * rows]


def gate_up(scaled, w_gate, w_up, extra, tail, layer, lo, hi, blk, pieces):
    tokens, depth = scaled.shape
    cut = (hi - lo) * blk
    rows = tokens // pieces
    wide = 2 * cut + (LANES if tail else 0)
    vmem = pl.BlockSpec(memory_space=pltpu.VMEM)
    hbm = pl.BlockSpec(memory_space=pl.ANY)
    return pl.pallas_call(
        lambda *refs: gate_up_kernel(*refs, layer=layer, lo=lo, blk=blk, cut=cut, tail=tail),
        in_specs=[vmem, hbm, hbm, vmem if tail else hbm],
        out_specs=[vmem] * pieces,
        out_shape=[jax.ShapeDtypeStruct((rows, wide), BF)] * pieces,
        scratch_shapes=[pltpu.VMEM((hi - lo, 2, depth, blk), F32), pltpu.SemaphoreType.DMA((hi - lo, 2))],
        cost_estimate=pl.CostEstimate(
            flops=4 * tokens * depth * cut, bytes_accessed=8 * depth * cut, transcendentals=0
        ),
    )(scaled, w_gate, w_up, extra)


def down_kernel(h_ref, w_hbm, *rest, layer, lo, blk, count):
    out, buf, sems = rest[-3:]
    copies = fetch(
        [
            pltpu.make_async_copy(w_hbm.at[layer, pl.ds((lo + j) * blk, blk)], buf.at[j], sems.at[j])
            for j in range(count)
        ]
    )
    total = rest[0][...] if len(rest) == 4 else None
    for j in range(count):
        copies[j].wait()
        value = jnp.dot(h_ref[:, j * blk : (j + 1) * blk], buf[j].astype(BF), preferred_element_type=F32)
        total = value if total is None else total + value
    out[...] = total.astype(out.dtype)


def down(hidden, w_down, layer, lo, hi, blk, before, dtype):
    tokens = hidden.shape[0]
    width = w_down.shape[2]
    vmem = pl.BlockSpec(memory_space=pltpu.VMEM)
    return pl.pallas_call(
        lambda *refs: down_kernel(*refs, layer=layer, lo=lo, blk=blk, count=hi - lo),
        in_specs=[vmem, pl.BlockSpec(memory_space=pl.ANY)] + ([] if before is None else [vmem]),
        out_specs=vmem,
        out_shape=jax.ShapeDtypeStruct((tokens, width), dtype),
        scratch_shapes=[pltpu.VMEM((hi - lo, blk, width), F32), pltpu.SemaphoreType.DMA((hi - lo,))],
        cost_estimate=pl.CostEstimate(
            flops=2 * tokens * width * (hi - lo) * blk,
            bytes_accessed=4 * width * (hi - lo) * blk,
            transcendentals=0,
        ),
    )(hidden, w_down, *(() if before is None else (before,)))


def ra_sum(squares):
    for bit in stages("ra"):
        squares = squares + swap(squares, "ra", bit)
    return squares


def cb_sum(mine):
    size = lax.axis_size("cb")
    if size == 1:
        return mine.astype(F32)
    pair = mine.astype(F32) + swap(mine, "cb", 1).astype(F32)
    if size == 2:
        return pair
    sent = pair.astype(BF)
    total = sent.astype(F32)
    for step in range(2, size, 2):
        total = total + shift(sent, "cb", step).astype(F32)
    return total


def local(stream, w_gate, w_up, w_down, gate_scale, up_scale, down_scale, pre_gain, out_gain):
    layers, width, ff = w_gate.shape
    tokens = stream.shape[0]
    parts = lax.axis_size("ra")
    features = width * parts
    share = tokens // parts
    bits = stages("ra")
    me = lax.axis_index("ra")
    home = sum(((me // bit) % 2) * bits[-1 - s] for s, bit in enumerate(bits))

    def reorder(value):
        if parts == 1:
            return value
        return jnp.concatenate(
            [lax.dynamic_slice_in_dim(value, (p ^ home) * share, share, 0) for p in range(parts)], axis=0
        )

    blk = column_block(ff)
    bounds = chunk_bounds(ff // blk)
    current = reorder(stream)
    for layer in range(layers):
        xvals = current.astype(F32)
        scaled = (xvals * pre_gain[layer]).astype(BF)
        extra = two_floats(jnp.sum(xvals * xvals, axis=1, keepdims=True))
        products = []
        for lo, hi in bounds:
            product = gate_up(scaled, w_gate, w_up, extra, lo == 0, layer, lo, hi, blk, 2 if bits else 1)
            products.append(product)
            extra = product[0]
        terms = None
        for (lo, hi), product in zip(bounds, products):
            cut = (hi - lo) * blk
            cols = slice(lo * blk, hi * blk)
            keep = product[0].astype(F32)
            send = product[-1]
            for s, bit in enumerate(bits):
                taken = swap(send, "ra", bit)
                keep = keep + taken.astype(F32)
                if s + 1 < len(bits):
                    half = keep.shape[0] // 2
                    send = keep[half:, : 2 * cut].astype(BF)
                    if lo == 0:
                        squares = jnp.sum(keep[half:, 2 * cut :], axis=1, keepdims=True)
                        send = jnp.concatenate([send, two_floats(squares)], axis=1)
                    keep = keep[:half]
            if lo == 0:
                total = jnp.sum(keep[:, 2 * cut :], axis=1, keepdims=True)
                rinv = lax.rsqrt(total / features + 1e-06)
            gate = keep[:, :cut] * rinv * gate_scale[layer, cols]
            upper = keep[:, cut : 2 * cut] * rinv * up_scale[layer, cols]
            hidden = (jax.nn.silu(gate) * upper).astype(BF)
            for s, bit in reversed(list(enumerate(bits))):
                taken = swap(hidden, "ra", bit)
                hidden = jnp.concatenate([hidden, taken], axis=0)
            last = hi == bounds[-1][1]
            terms = down(hidden, w_down, layer, lo, hi, blk, terms, BF if last else F32)
        branch = cb_sum(terms) * down_scale[layer]
        current = (0.5 * xvals + branch).astype(BF)
    xvals = reorder(current).astype(F32)
    final_sum = ra_sum(jnp.sum(xvals * xvals, axis=1))
    rinv = lax.rsqrt(final_sum / features + 1e-06)[:, None]
    return (xvals * rinv * out_gain).astype(BF)


def solution(mesh):
    placed = (
        P("grp", "ra"),
        P(None, "ra", "cb"),
        P(None, "ra", "cb"),
        P(None, "cb", "ra"),
        P(None, "cb"),
        P(None, "cb"),
        P(None, "ra"),
        P(None, "ra"),
        P("ra"),
    )
    return jax.shard_map(
        local, mesh=mesh, in_specs=placed, out_specs=P("grp", "ra"), check_vma=False
    )
```

time: 298 us -> 190 us (0.64)
  blocking collectives: 71.9 us -> 0 us
  Pallas kernels: 0 us -> 45.5 us
  waiting for transfers between devices: 143 us -> 106 us
  other arithmetic: 36.8 us -> 13.2 us
  matrix products: 22 us -> 0 us
  starting transfers between devices: 0.21 us -> 21.8 us
  between operations: 13.6 us -> 0.38 us
  local copies, waits for them, and re-layouts: 9.34 us -> 2.02 us
    ppermute x0 -> x22, waiting for transfers between devices: none -> 106 us  [the longest x20 91.1 us: swap(): return lax.ppermute(value, axis, [(i, i ^ bit) for i in range(size)])]
    reduce_scatter x4 -> x0, waiting for transfers between devices: 80.2 us -> none  [the longest x2 63.6 us: local(): lax.psum_scatter(operands[1], 'ra', scatter_dimension=0, tiled=True)]
    psum x2 -> x0, waiting for transfers between devices: 62.8 us -> none  [local(): lax.psum(terms.astype(jnp.bfloat16), 'cb').astype(jnp.float32)]
    pallas_call x0 -> x8, Pallas kernels: none -> 45.5 us  [the longest x4 26.5 us: gate_up(): pl.pallas_call(lambda *refs: gate_up_kernel(*refs, layer=layer, lo=lo, bl...]
    psum x3 -> x0, blocking collectives: 37.6 us -> none  [the longest x2 25.9 us: local(): total = lax.psum(squares, 'ra')]
    all_gather x2 -> x0, blocking collectives: 34.3 us -> none  [local(): lax.all_gather(hidden, 'ra', axis=0, tiled=True)]
    another operation x3 -> x0, other arithmetic: 29.8 us -> none
    dot_general x6 -> x0, matrix products: 22 us -> none  [the longest x2 8.61 us: local(): jnp.dot(lax.all_gather(hidden, 'ra', axis=0, tiled=True), down_local, pre...]
  transfers between devices with their start and end apart: 6 -> 22, of which waited for: 5 -> 20; matrix products, arithmetic and copies ran while one was open for 10% -> 3% of each run, Pallas kernels for 0% -> 0%
where the time goes in v1:
time: 190 us; the launch traced here: 189 us
  waiting for transfers between devices  106 us (56%)
  Pallas kernels  45.5 us (24%)
  starting transfers between devices  21.8 us (11%)
  other arithmetic  13.2 us (7%)
  local copies, waits for them, and re-layouts  2.02 us (1%)
    ppermute x20, waiting for transfers between devices, swap(): return lax.ppermute(value, axis, [(i, i ^ bit) for i in range(size)])  91.1 us
    pallas_call x4, Pallas kernels, gate_up(): pl.pallas_call(lambda *refs: gate_up_kernel(*refs, layer=layer, lo=lo, bl...  26.5 us
    ppermute x20, starting transfers between devices, swap(): return lax.ppermute(value, axis, [(i, i ^ bit) for i in range(size)])  20 us
    pallas_call x4, Pallas kernels, down(): pl.pallas_call(lambda *refs: down_kernel(*refs, layer=layer, lo=lo, blk=b...  19 us
    ppermute x2, waiting for transfers between devices, shift(): lax.ppermute(value, axis, [(i, (i + step) % size) for i in range(size)])  15 us
  transfers between devices with their start and end apart: 22, of which 20 were waited for; matrix products, arithmetic and copies ran while one was open for 3% of the time, Pallas kernels for 0%

profile of v1, /device:TPU:0, one launch (start us, length us, event | category | flops | bytes accessed | tf_op | source)
XLA Modules:
  0.0 189.0 jit_solution(8684358733452541019)
XLA Ops:
  0.0 0.8 fusion.29
  0.8 1.0 constant_dynamic-slice_fusion.7
  1.8 0.8 fusion.6
  2.6 0.7 select_convert_fusion.1.refs_3_
  3.3 6.9 %shard_map.91 = (bf16[64,3200]{1,0:T(8,128)(2,1)}, bf16[64,3200]{1,0:T(8,128)(2,1)}) custom-call(bf16[128,1024]{1,0:T(8,128)(2,1)} %get-tuple-element.36.refs_0_, f32[2,1024,2816]{2,1,0:T(8,128)} %refs_1_.13, f32[2,1024,2816]{2,1,0:T(8,128)} %refs_2_.7, bf16[128,128]{1,0:T(8,128)(2,1)} %select_convert_fusion.1.refs_3_), custom_call_target="tpu_custom_call" | custom-call | flops 805306368 | bytes 12582912 | tf_op jit(solution)/shard_map/pallas_call | solution.py:88
  10.3 6.3 %shard_map.92 = (bf16[64,2560]{1,0:T(8,128)(2,1)}, bf16[64,2560]{1,0:T(8,128)(2,1)}) custom-call(bf16[128,1024]{1,0:T(8,128)(2,1)} %get-tuple-element.36.refs_0_, f32[2,1024,2816]{2,1,0:T(8,128)} %refs_1_.13, f32[2,1024,2816]{2,1,0:T(8,128)} %refs_2_.7, bf16[64,3200]{1,0:T(8,128)(2,1)} %get-tuple-element.13.refs_3_), custom_call_target="tpu_custom_call" | custom-call | flops 671088640 | bytes 10485760 | tf_op jit(solution)/shard_map/pallas_call | solution.py:88
  16.6 3.1 %collective-permute-start = (bf16[64,2560]{1,0:T(8,128)(2,1)}, bf16[64,2560]{1,0:T(8,128)(2,1)S(1)}, u32[]{:S(2)}, u32[]{:S(2)}) collective-permute-start(bf16[64,2560]{1,0:T(8,128)(2,1)} %get-tuple-element.15), channel_id=1, source_target_pairs={{0,4},{4,0},{8,12},{12,8},{1,5},{5,1},{9,13},{13,9},{2,6},{6,2},{1... | collective-permute-start | bytes 983048 | tf_op jit(solution)/shard_map/ppermute | solution.py:22
  19.9 8.6 %collective-permute-done = bf16[64,2560]{1,0:T(8,128)(2,1)S(1)} collective-permute-done((bf16[64,2560]{1,0:T(8,128)(2,1)}, bf16[64,2560]{1,0:T(8,128)(2,1)S(1)}, u32[]{:S(2)}, u32[]{:S(2)}) %collective-permute-start) | collective-permute-done | bytes 327712 | tf_op jit(solution)/shard_map/ppermute | solution.py:22
  28.5 1.0 convert_add_fusion.3
  29.6 3.1 %collective-permute-start.1 = (bf16[32,2560]{1,0:T(8,128)(2,1)S(1)}, bf16[32,2560]{1,0:T(8,128)(2,1)S(1)}, u32[]{:S(2)}, u32[]{:S(2)}) collective-permute-start(bf16[32,2560]{1,0:T(8,128)(2,1)S(1)} %slice.223), channel_id=1, source_target_pairs={{0,8},{4,12},{8,0},{12,4},{1,9},{5,13},{9,1},{13,5},{2,10},{6,14},... | collective-permute-start | bytes 491528 | tf_op jit(solution)/shard_map/ppermute | solution.py:22
  32.7 7.3 %collective-permute-done.2 = bf16[64,3200]{1,0:T(8,128)(2,1)S(1)} collective-permute-done((bf16[64,3200]{1,0:T(8,128)(2,1)S(1)}, bf16[64,3200]{1,0:T(8,128)(2,1)S(1)}, u32[]{:S(2)}, u32[]{:S(2)}) %collective-permute-start.2) | collective-permute-done | bytes 409632 | tf_op jit(solution)/shard_map/ppermute | solution.py:22
  40.3 1.9 %collective-permute-start.3 = (bf16[32,3200]{1,0:T(8,128)(2,1)S(1)}, bf16[32,3200]{1,0:T(8,128)(2,1)S(1)}, u32[]{:S(2)}, u32[]{:S(2)}) collective-permute-start(bf16[32,3200]{1,0:T(8,128)(2,1)S(1)} %pad_maximum_fusion.6), channel_id=1, source_target_pairs={{0,8},{4,12},{8,0},{12,4},{1,9},{5,13},{9,1},{13,5},{2,10},{6,14},... | collective-permute-start | bytes 614408 | tf_op jit(solution)/shard_map/ppermute | solution.py:22
  42.2 9.6 %collective-permute-done.3 = bf16[32,3200]{1,0:T(8,128)(2,1)S(1)} collective-permute-done((bf16[32,3200]{1,0:T(8,128)(2,1)S(1)}, bf16[32,3200]{1,0:T(8,128)(2,1)S(1)}, u32[]{:S(2)}, u32[]{:S(2)}) %collective-permute-start.3) | collective-permute-done | bytes 204832 | tf_op jit(solution)/shard_map/ppermute | solution.py:22
  52.0 0.1 fusion.25
  52.3 0.1 fusion.17
  52.4 3.0 %collective-permute-start.6 = (bf16[32,1536]{1,0:T(8,128)(2,1)S(1)}, bf16[32,1536]{1,0:T(8,128)(2,1)S(1)}, u32[]{:S(2)}, u32[]{:S(2)}) collective-permute-start(bf16[32,1536]{1,0:T(8,128)(2,1)S(1)} %fusion.17), channel_id=1, source_target_pairs={{0,8},{4,12},{8,0},{12,4},{1,9},{5,13},{9,1},{13,5},{2,10},{6,14},... | collective-permute-start | bytes 294920 | tf_op jit(solution)/shard_map/ppermute | solution.py:22
  55.4 6.0 %collective-permute-done.4 = bf16[32,1280]{1,0:T(8,128)(2,1)S(1)} collective-permute-done((bf16[32,1280]{1,0:T(8,128)(2,1)S(1)}, bf16[32,1280]{1,0:T(8,128)(2,1)S(1)}, u32[]{:S(2)}, u32[]{:S(2)}) %collective-permute-start.4) | collective-permute-done | bytes 81952 | tf_op jit(solution)/shard_map/ppermute | solution.py:22
  61.5 1.2 collective-permute-done.6
  62.8 0.8 collective-permute-start.7
  63.6 5.0 %collective-permute-done.5 = bf16[64,1280]{1,0:T(8,128)(2,1)S(1)} collective-permute-done((bf16[64,1280]{1,0:T(8,128)(2,1)S(1)}, bf16[64,1280]{1,0:T(8,128)(2,1)S(1)}, u32[]{:S(2)}, u32[]{:S(2)}) %collective-permute-start.5) | collective-permute-done | bytes 163872 | tf_op jit(solution)/shard_map/ppermute | solution.py:22
  68.6 0.8 pad_maximum_fusion.2.refs_0_
  69.3 1.3 collective-permute-done.7
  70.7 0.8 pad_maximum_fusion.refs_0_
  71.4 4.9 %shard_map.93.refs_2_ = f32[128,1024]{1,0:T(8,128)} custom-call(bf16[128,1536]{1,0:T(8,128)(2,1)} %pad_maximum_fusion.refs_0_, f32[2,2816,1024]{2,1,0:T(8,128)} %refs_1_.15), custom_call_target="tpu_custom_call" | custom-call | flops 402653184 | bytes 6291456 | tf_op jit(solution)/shard_map/pallas_call | solution.py:120
  76.3 4.6 %shard_map.94 = bf16[128,1024]{1,0:T(8,128)(2,1)} custom-call(bf16[128,1280]{1,0:T(8,128)(2,1)} %pad_maximum_fusion.2.refs_0_, f32[2,2816,1024]{2,1,0:T(8,128)} %refs_1_.15, f32[128,1024]{1,0:T(8,128)} %shard_map.93.refs_2_), custom_call_target="tpu_custom_call" | custom-call | flops 335544320 | bytes 5242880 | tf_op jit(solution)/shard_map/pallas_call | solution.py:120
  81.0 1.7 collective-permute-done.8
  82.8 1.0 add_convert_fusion.1
  83.8 1.0 collective-permute-start.9
  84.8 7.4 %collective-permute-done.9 = bf16[128,1024]{1,0:T(8,128)(2,1)S(1)} collective-permute-done((bf16[128,1024]{1,0:T(8,128)(2,1)S(1)}, bf16[128,1024]{1,0:T(8,128)(2,1)S(1)}, u32[]{:S(2)}, u32[]{:S(2)}) %collective-permute-start.9) | collective-permute-done | bytes 262176 | tf_op jit(solution)/shard_map/ppermute | solution.py:17
  92.2 0.2 fusion.10
  92.5 0.8 fusion.9.refs_0_
  93.2 0.7 select_convert_fusion.refs_3_
  93.9 6.9 %shard_map.95 = (bf16[64,3200]{1,0:T(8,128)(2,1)}, bf16[64,3200]{1,0:T(8,128)(2,1)}) custom-call(bf16[128,1024]{1,0:T(8,128)(2,1)} %fusion.9.refs_0_, f32[2,1024,2816]{2,1,0:T(8,128)} %refs_1_.13, f32[2,1024,2816]{2,1,0:T(8,128)} %refs_2_.7, bf16[128,128]{1,0:T(8,128)(2,1)} %select_convert_fusion.refs_3_), custom_call_target="tpu_custom_call" | custom-call | flops 805306368 | bytes 12582912 | tf_op jit(solution)/shard_map/pallas_call | solution.py:88
  100.9 6.3 %shard_map.96 = (bf16[64,2560]{1,0:T(8,128)(2,1)}, bf16[64,2560]{1,0:T(8,128)(2,1)}) custom-call(bf16[128,1024]{1,0:T(8,128)(2,1)} %fusion.9.refs_0_, f32[2,1024,2816]{2,1,0:T(8,128)} %refs_1_.13, f32[2,1024,2816]{2,1,0:T(8,128)} %refs_2_.7, bf16[64,3200]{1,0:T(8,128)(2,1)} %get-tuple-element.17.refs_3_), custom_call_target="tpu_custom_call" | custom-call | flops 671088640 | bytes 10485760 | tf_op jit(solution)/shard_map/pallas_call | solution.py:88
  107.2 0.4 collective-permute-start.10
  107.6 1.7 collective-permute-start.12
  109.3 8.8 %collective-permute-done.10 = bf16[64,2560]{1,0:T(8,128)(2,1)S(1)} collective-permute-done((bf16[64,2560]{1,0:T(8,128)(2,1)}, bf16[64,2560]{1,0:T(8,128)(2,1)S(1)}, u32[]{:S(2)}, u32[]{:S(2)}) %collective-permute-start.10) | collective-permute-done | bytes 327712 | tf_op jit(solution)/shard_map/ppermute | solution.py:22
  118.1 1.0 convert_add_fusion.2
  119.1 0.9 collective-permute-start.11
  120.1 8.6 %collective-permute-done.12 = bf16[64,3200]{1,0:T(8,128)(2,1)S(1)} collective-permute-done((bf16[64,3200]{1,0:T(8,128)(2,1)S(1)}, bf16[64,3200]{1,0:T(8,128)(2,1)S(1)}, u32[]{:S(2)}, u32[]{:S(2)}) %collective-permute-start.12) | collective-permute-done | bytes 409632 | tf_op jit(solution)/shard_map/ppermute | solution.py:22
  129.0 0.1 collective-permute-start.13
  129.2 9.8 %collective-permute-done.13 = bf16[32,3200]{1,0:T(8,128)(2,1)S(1)} collective-permute-done((bf16[32,3200]{1,0:T(8,128)(2,1)S(1)}, bf16[32,3200]{1,0:T(8,128)(2,1)S(1)}, u32[]{:S(2)}, u32[]{:S(2)}) %collective-permute-start.13) | collective-permute-done | bytes 204832 | tf_op jit(solution)/shard_map/ppermute | solution.py:22
  139.2 0.1 fusion.21
  139.3 0.3 collective-permute-start.14
  139.6 0.1 fusion.13
  139.7 3.0 %collective-permute-start.16 = (bf16[32,1536]{1,0:T(8,128)(2,1)S(1)}, bf16[32,1536]{1,0:T(8,128)(2,1)S(1)}, u32[]{:S(2)}, u32[]{:S(2)}) collective-permute-start(bf16[32,1536]{1,0:T(8,128)(2,1)S(1)} %fusion.13), channel_id=1, source_target_pairs={{0,8},{4,12},{8,0},{12,4},{1,9},{5,13},{9,1},{13,5},{2,10},{6,14},... | collective-permute-start | bytes 294920 | tf_op jit(solution)/shard_map/ppermute | solution.py:22
  142.7 5.2 %collective-permute-done.14 = bf16[32,1280]{1,0:T(8,128)(2,1)S(1)} collective-permute-done((bf16[32,1280]{1,0:T(8,128)(2,1)S(1)}, bf16[32,1280]{1,0:T(8,128)(2,1)S(1)}, u32[]{:S(2)}, u32[]{:S(2)}) %collective-permute-start.14) | collective-permute-done | bytes 81952 | tf_op jit(solution)/shard_map/ppermute | solution.py:22
  148.0 1.9 %collective-permute-done.16 = bf16[32,1536]{1,0:T(8,128)(2,1)S(1)} collective-permute-done((bf16[32,1536]{1,0:T(8,128)(2,1)S(1)}, bf16[32,1536]{1,0:T(8,128)(2,1)S(1)}, u32[]{:S(2)}, u32[]{:S(2)}) %collective-permute-start.16) | collective-permute-done | bytes 98336 | tf_op jit(solution)/shard_map/ppermute | solution.py:22
  149.9 0.2 collective-permute-start.17
  150.1 5.0 %collective-permute-done.15 = bf16[64,1280]{1,0:T(8,128)(2,1)S(1)} collective-permute-done((bf16[64,1280]{1,0:T(8,128)(2,1)S(1)}, bf16[64,1280]{1,0:T(8,128)(2,1)S(1)}, u32[]{:S(2)}, u32[]{:S(2)}) %collective-permute-start.15) | collective-permute-done | bytes 163872 | tf_op jit(solution)/shard_map/ppermute | solution.py:22
  155.0 0.8 pad_maximum_fusion.3.refs_0_
  155.8 2.4 %collective-permute-done.17 = bf16[64,1536]{1,0:T(8,128)(2,1)S(1)} collective-permute-done((bf16[64,1536]{1,0:T(8,128)(2,1)S(1)}, bf16[64,1536]{1,0:T(8,128)(2,1)S(1)}, u32[]{:S(2)}, u32[]{:S(2)}) %collective-permute-start.17) | collective-permute-done | bytes 196640 | tf_op jit(solution)/shard_map/ppermute | solution.py:22
  158.2 0.8 pad_maximum_fusion.1.refs_0_
  159.0 4.9 %shard_map.97.refs_2_ = f32[128,1024]{1,0:T(8,128)} custom-call(bf16[128,1536]{1,0:T(8,128)(2,1)} %pad_maximum_fusion.1.refs_0_, f32[2,2816,1024]{2,1,0:T(8,128)} %refs_1_.15), custom_call_target="tpu_custom_call" | custom-call | flops 402653184 | bytes 6291456 | tf_op jit(solution)/shard_map/pallas_call | solution.py:120
  163.9 4.6 %shard_map.98 = bf16[128,1024]{1,0:T(8,128)(2,1)} custom-call(bf16[128,1280]{1,0:T(8,128)(2,1)} %pad_maximum_fusion.3.refs_0_, f32[2,2816,1024]{2,1,0:T(8,128)} %refs_1_.15, f32[128,1024]{1,0:T(8,128)} %shard_map.97.refs_2_), custom_call_target="tpu_custom_call" | custom-call | flops 335544320 | bytes 5242880 | tf_op jit(solution)/shard_map/pallas_call | solution.py:120
  168.6 1.7 collective-permute-done.18
  170.3 1.0 add_convert_fusion
  171.3 0.7 collective-permute-start.19
  172.1 7.7 %collective-permute-done.19 = bf16[128,1024]{1,0:T(8,128)(2,1)S(1)} collective-permute-done((bf16[128,1024]{1,0:T(8,128)(2,1)S(1)}, bf16[128,1024]{1,0:T(8,128)(2,1)S(1)}, u32[]{:S(2)}, u32[]{:S(2)}) %collective-permute-start.19) | collective-permute-done | bytes 262176 | tf_op jit(solution)/shard_map/ppermute | solution.py:17
  180.1 0.3 collective-permute-start.20
  180.4 3.3 %collective-permute-done.20 = f32[128]{0:T(128)S(1)} collective-permute-done((f32[128]{0:T(128)S(1)}, f32[128]{0:T(128)S(1)}, u32[]{:S(2)}, u32[]{:S(2)}) %collective-permute-start.20) | collective-permute-done | bytes 544 | tf_op jit(solution)/shard_map/ppermute | solution.py:22
  183.7 0.8 collective-permute-start.21
  184.5 3.7 %collective-permute-done.21 = f32[128]{0:T(128)S(1)} collective-permute-done((f32[128]{0:T(128)S(1)}, f32[128]{0:T(128)S(1)}, u32[]{:S(2)}, u32[]{:S(2)}) %collective-permute-start.21) | collective-permute-done | bytes 544 | tf_op jit(solution)/shard_map/ppermute | solution.py:22
  188.2 0.8 fusion.2
  (62 shorter events, 2.1 us)
Async XLA Ops:
  10.2 9.5 %copy-start.6 = (bf16[64,3200]{1,0:T(8,128)(2,1)S(1)}, bf16[64,3200]{1,0:T(8,128)(2,1)}, u32[]{:S(2)}) copy-start(bf16[64,3200]{1,0:T(8,128)(2,1)} %get-tuple-element.16) | copy-start | bytes 1228804
  10.2 9.6 %copy-start.2 = (f32[2,2816]{1,0:T(2,128)S(1)}, f32[2,2816]{1,0:T(2,128)}, u32[]{:S(2)}) copy-start(f32[2,2816]{1,0:T(2,128)} %param.14) | copy-start | bytes 67588
  10.3 9.6 %copy-start.3 = (f32[2,2816]{1,0:T(2,128)S(1)}, f32[2,2816]{1,0:T(2,128)}, u32[]{:S(2)}) copy-start(f32[2,2816]{1,0:T(2,128)} %param.13) | copy-start | bytes 67588
  10.3 29.7 %copy-start = (bf16[64,3200]{1,0:T(8,128)(2,1)S(1)}, bf16[64,3200]{1,0:T(8,128)(2,1)}, u32[]{:S(2)}) copy-start(bf16[64,3200]{1,0:T(8,128)(2,1)} %get-tuple-element.13.refs_3_) | copy-start | bytes 1228804
  16.6 11.9 %collective-permute-start = (bf16[64,2560]{1,0:T(8,128)(2,1)}, bf16[64,2560]{1,0:T(8,128)(2,1)S(1)}, u32[]{:S(2)}, u32[]{:S(2)}) collective-permute-start(bf16[64,2560]{1,0:T(8,128)(2,1)} %get-tuple-element.15), channel_id=1, source_target_pairs={{0,4},{4,0},{8,12},{12,8},{1,5},{5,1},{9,13},{13,9},{2,6},{6,2},{1... | collective-permute-start | bytes 983048 | tf_op jit(solution)/shard_map/ppermute | solution.py:22
  19.7 20.2 %collective-permute-start.2 = (bf16[64,3200]{1,0:T(8,128)(2,1)S(1)}, bf16[64,3200]{1,0:T(8,128)(2,1)S(1)}, u32[]{:S(2)}, u32[]{:S(2)}) collective-permute-start(bf16[64,3200]{1,0:T(8,128)(2,1)S(1)} %copy-done.6), channel_id=1, source_target_pairs={{0,4},{4,0},{8,12},{12,8},{1,5},{5,1},{9,13},{13,9},{2,6},{6,2},{1... | collective-permute-start | bytes 1228808 | tf_op jit(solution)/shard_map/ppermute | solution.py:22
  29.6 12.6 %collective-permute-start.1 = (bf16[32,2560]{1,0:T(8,128)(2,1)S(1)}, bf16[32,2560]{1,0:T(8,128)(2,1)S(1)}, u32[]{:S(2)}, u32[]{:S(2)}) collective-permute-start(bf16[32,2560]{1,0:T(8,128)(2,1)S(1)} %slice.223), channel_id=1, source_target_pairs={{0,8},{4,12},{8,0},{12,4},{1,9},{5,13},{9,1},{13,5},{2,10},{6,14},... | collective-permute-start | bytes 491528 | tf_op jit(solution)/shard_map/ppermute | solution.py:22
  40.3 11.6 %collective-permute-start.3 = (bf16[32,3200]{1,0:T(8,128)(2,1)S(1)}, bf16[32,3200]{1,0:T(8,128)(2,1)S(1)}, u32[]{:S(2)}, u32[]{:S(2)}) collective-permute-start(bf16[32,3200]{1,0:T(8,128)(2,1)S(1)} %pad_maximum_fusion.6), channel_id=1, source_target_pairs={{0,8},{4,12},{8,0},{12,4},{1,9},{5,13},{9,1},{13,5},{2,10},{6,14},... | collective-permute-start | bytes 614408 | tf_op jit(solution)/shard_map/ppermute | solution.py:22
  52.2 9.2 %collective-permute-start.4 = (bf16[32,1280]{1,0:T(8,128)(2,1)S(1)}, bf16[32,1280]{1,0:T(8,128)(2,1)S(1)}, u32[]{:S(2)}, u32[]{:S(2)}) collective-permute-start(bf16[32,1280]{1,0:T(8,128)(2,1)S(1)} %fusion.25), channel_id=1, source_target_pairs={{0,8},{4,12},{8,0},{12,4},{1,9},{5,13},{9,1},{13,5},{2,10},{6,14},... | collective-permute-start | bytes 245768 | tf_op jit(solution)/shard_map/ppermute | solution.py:22
  52.4 10.3 %collective-permute-start.6 = (bf16[32,1536]{1,0:T(8,128)(2,1)S(1)}, bf16[32,1536]{1,0:T(8,128)(2,1)S(1)}, u32[]{:S(2)}, u32[]{:S(2)}) collective-permute-start(bf16[32,1536]{1,0:T(8,128)(2,1)S(1)} %fusion.17), channel_id=1, source_target_pairs={{0,8},{4,12},{8,0},{12,4},{1,9},{5,13},{9,1},{13,5},{2,10},{6,14},... | collective-permute-start | bytes 294920 | tf_op jit(solution)/shard_map/ppermute | solution.py:22
  61.4 7.1 %collective-permute-start.5 = (bf16[64,1280]{1,0:T(8,128)(2,1)S(1)}, bf16[64,1280]{1,0:T(8,128)(2,1)S(1)}, u32[]{:S(2)}, u32[]{:S(2)}) collective-permute-start(bf16[64,1280]{1,0:T(8,128)(2,1)S(1)} %pad_maximum_fusion.10), channel_id=1, source_target_pairs={{0,4},{4,0},{8,12},{12,8},{1,5},{5,1},{9,13},{13,9},{2,6},{6,2},{1... | collective-permute-start | bytes 491528 | tf_op jit(solution)/shard_map/ppermute | solution.py:22
  62.8 7.9 %collective-permute-start.7 = (bf16[64,1536]{1,0:T(8,128)(2,1)S(1)}, bf16[64,1536]{1,0:T(8,128)(2,1)S(1)}, u32[]{:S(2)}, u32[]{:S(2)}) collective-permute-start(bf16[64,1536]{1,0:T(8,128)(2,1)S(1)} %pad_maximum_fusion.8), channel_id=1, source_target_pairs={{0,4},{4,0},{8,12},{12,8},{1,5},{5,1},{9,13},{13,9},{2,6},{6,2},{1... | collective-permute-start | bytes 589832 | tf_op jit(solution)/shard_map/ppermute | solution.py:22
  71.4 13.4 %copy-start.4 = (f32[2,1024]{1,0:T(2,128)S(1)}, f32[2,1024]{1,0:T(2,128)}, u32[]{:S(2)}) copy-start(f32[2,1024]{1,0:T(2,128)} %param.15) | copy-start | bytes 24580
  81.0 1.8 collective-permute-start.8
  83.8 8.4 %collective-permute-start.9 = (bf16[128,1024]{1,0:T(8,128)(2,1)S(1)}, bf16[128,1024]{1,0:T(8,128)(2,1)S(1)}, u32[]{:S(2)}, u32[]{:S(2)}) collective-permute-start(bf16[128,1024]{1,0:T(8,128)(2,1)S(1)} %add_convert_fusion.1), channel_id=1, source_target_pairs={{0,2},{1,3},{2,0},{3,1},{4,6},{5,7},{6,4},{7,5},{8,10},{9,11},{10,... | collective-permute-start | bytes 786440 | tf_op jit(solution)/shard_map/ppermute | solution.py:17
  100.9 6.7 %copy-start.7 = (bf16[64,3200]{1,0:T(8,128)(2,1)S(1)}, bf16[64,3200]{1,0:T(8,128)(2,1)}, u32[]{:S(2)}) copy-start(bf16[64,3200]{1,0:T(8,128)(2,1)} %get-tuple-element.20) | copy-start | bytes 1228804
  100.9 27.8 %copy-start.1 = (bf16[64,3200]{1,0:T(8,128)(2,1)S(1)}, bf16[64,3200]{1,0:T(8,128)(2,1)}, u32[]{:S(2)}) copy-start(bf16[64,3200]{1,0:T(8,128)(2,1)} %get-tuple-element.17.refs_3_) | copy-start | bytes 1228804
  107.2 10.9 %collective-permute-start.10 = (bf16[64,2560]{1,0:T(8,128)(2,1)}, bf16[64,2560]{1,0:T(8,128)(2,1)S(1)}, u32[]{:S(2)}, u32[]{:S(2)}) collective-permute-start(bf16[64,2560]{1,0:T(8,128)(2,1)} %get-tuple-element.19), channel_id=1, source_target_pairs={{0,4},{4,0},{8,12},{12,8},{1,5},{5,1},{9,13},{13,9},{2,6},{6,2},{1... | collective-permute-start | bytes 983048 | tf_op jit(solution)/shard_map/ppermute | solution.py:22
  107.6 21.1 %collective-permute-start.12 = (bf16[64,3200]{1,0:T(8,128)(2,1)S(1)}, bf16[64,3200]{1,0:T(8,128)(2,1)S(1)}, u32[]{:S(2)}, u32[]{:S(2)}) collective-permute-start(bf16[64,3200]{1,0:T(8,128)(2,1)S(1)} %copy-done.7), channel_id=1, source_target_pairs={{0,4},{4,0},{8,12},{12,8},{1,5},{5,1},{9,13},{13,9},{2,6},{6,2},{1... | collective-permute-start | bytes 1228808 | tf_op jit(solution)/shard_map/ppermute | solution.py:22
  119.1 10.0 %collective-permute-start.11 = (bf16[32,2560]{1,0:T(8,128)(2,1)S(1)}, bf16[32,2560]{1,0:T(8,128)(2,1)S(1)}, u32[]{:S(2)}, u32[]{:S(2)}) collective-permute-start(bf16[32,2560]{1,0:T(8,128)(2,1)S(1)} %slice.222), channel_id=1, source_target_pairs={{0,8},{4,12},{8,0},{12,4},{1,9},{5,13},{9,1},{13,5},{2,10},{6,14},... | collective-permute-start | bytes 491528 | tf_op jit(solution)/shard_map/ppermute | solution.py:22
  129.0 10.0 %collective-permute-start.13 = (bf16[32,3200]{1,0:T(8,128)(2,1)S(1)}, bf16[32,3200]{1,0:T(8,128)(2,1)S(1)}, u32[]{:S(2)}, u32[]{:S(2)}) collective-permute-start(bf16[32,3200]{1,0:T(8,128)(2,1)S(1)} %pad_maximum_fusion.7), channel_id=1, source_target_pairs={{0,8},{4,12},{8,0},{12,4},{1,9},{5,13},{9,1},{13,5},{2,10},{6,14},... | collective-permute-start | bytes 614408 | tf_op jit(solution)/shard_map/ppermute | solution.py:22
  139.3 8.6 %collective-permute-start.14 = (bf16[32,1280]{1,0:T(8,128)(2,1)S(1)}, bf16[32,1280]{1,0:T(8,128)(2,1)S(1)}, u32[]{:S(2)}, u32[]{:S(2)}) collective-permute-start(bf16[32,1280]{1,0:T(8,128)(2,1)S(1)} %fusion.21), channel_id=1, source_target_pairs={{0,8},{4,12},{8,0},{12,4},{1,9},{5,13},{9,1},{13,5},{2,10},{6,14},... | collective-permute-start | bytes 245768 | tf_op jit(solution)/shard_map/ppermute | solution.py:22
  139.7 10.2 %collective-permute-start.16 = (bf16[32,1536]{1,0:T(8,128)(2,1)S(1)}, bf16[32,1536]{1,0:T(8,128)(2,1)S(1)}, u32[]{:S(2)}, u32[]{:S(2)}) collective-permute-start(bf16[32,1536]{1,0:T(8,128)(2,1)S(1)} %fusion.13), channel_id=1, source_target_pairs={{0,8},{4,12},{8,0},{12,4},{1,9},{5,13},{9,1},{13,5},{2,10},{6,14},... | collective-permute-start | bytes 294920 | tf_op jit(solution)/shard_map/ppermute | solution.py:22
  147.9 7.1 %collective-permute-start.15 = (bf16[64,1280]{1,0:T(8,128)(2,1)S(1)}, bf16[64,1280]{1,0:T(8,128)(2,1)S(1)}, u32[]{:S(2)}, u32[]{:S(2)}) collective-permute-start(bf16[64,1280]{1,0:T(8,128)(2,1)S(1)} %pad_maximum_fusion.11), channel_id=1, source_target_pairs={{0,4},{4,0},{8,12},{12,8},{1,5},{5,1},{9,13},{13,9},{2,6},{6,2},{1... | collective-permute-start | bytes 491528 | tf_op jit(solution)/shard_map/ppermute | solution.py:22
  149.9 8.3 %collective-permute-start.17 = (bf16[64,1536]{1,0:T(8,128)(2,1)S(1)}, bf16[64,1536]{1,0:T(8,128)(2,1)S(1)}, u32[]{:S(2)}, u32[]{:S(2)}) collective-permute-start(bf16[64,1536]{1,0:T(8,128)(2,1)S(1)} %pad_maximum_fusion.9), channel_id=1, source_target_pairs={{0,4},{4,0},{8,12},{12,8},{1,5},{5,1},{9,13},{13,9},{2,6},{6,2},{1... | collective-permute-start | bytes 589832 | tf_op jit(solution)/shard_map/ppermute | solution.py:22
  159.0 29.2 %copy-start.5 = (f32[1024]{0:T(1024)S(1)}, f32[1024]{0:T(1024)}, u32[]{:S(2)}) copy-start(f32[1024]{0:T(1024)} %param.17) | copy-start | bytes 12292
  168.5 1.8 collective-permute-start.18
  171.3 8.4 %collective-permute-start.19 = (bf16[128,1024]{1,0:T(8,128)(2,1)S(1)}, bf16[128,1024]{1,0:T(8,128)(2,1)S(1)}, u32[]{:S(2)}, u32[]{:S(2)}) collective-permute-start(bf16[128,1024]{1,0:T(8,128)(2,1)S(1)} %add_convert_fusion), channel_id=1, source_target_pairs={{0,2},{1,3},{2,0},{3,1},{4,6},{5,7},{6,4},{7,5},{8,10},{9,11},{10,... | collective-permute-start | bytes 786440 | tf_op jit(solution)/shard_map/ppermute | solution.py:17
  180.1 3.6 %collective-permute-start.20 = (f32[128]{0:T(128)S(1)}, f32[128]{0:T(128)S(1)}, u32[]{:S(2)}, u32[]{:S(2)}) collective-permute-start(f32[128]{0:T(128)S(1)} %fusion), channel_id=1, source_target_pairs={{0,4},{4,0},{8,12},{12,8},{1,5},{5,1},{9,13},{13,9},{2,6},{6,2},{1... | collective-permute-start | bytes 1544 | tf_op jit(solution)/shard_map/ppermute | solution.py:22
  183.7 4.5 %collective-permute-start.21 = (f32[128]{0:T(128)S(1)}, f32[128]{0:T(128)S(1)}, u32[]{:S(2)}, u32[]{:S(2)}) collective-permute-start(f32[128]{0:T(128)S(1)} %add.139), channel_id=1, source_target_pairs={{0,8},{4,12},{8,0},{12,4},{1,9},{5,13},{9,1},{13,5},{2,10},{6,14},... | collective-permute-start | bytes 1544 | tf_op jit(solution)/shard_map/ppermute | solution.py:22
